TPU v7x, 32 devices: a whole 2x2x4 slice. The times are simulated.
32 devices in a mesh: rep: 2 (over x), fs: 8 (over z, y), tp: 2 (over core).
Axes of the slice: x: 2, y: 2, z: 4, core: 2. Of those that a mesh axis runs over, the one named last changes fastest.
Arguments:
- tokens: bfloat16 [4096, 2048], P(('rep', 'fs'), 'tp'), may hold values from -30 to 30
- first_gain: float32 [2048], replicated, may hold values from 0.1 to 1.9
- up_weight: bfloat16 [2048, 1024], P('fs', 'tp'), may hold values from -0.125 to 0.125
- value_weight: bfloat16 [2048, 1024], P('fs', 'tp'), may hold values from -1 to 1
- value_gain: float32 [1024], P('tp'), may hold values from 0.1 to 1.9
- mix_weight: bfloat16 [8, 128, 128], P('tp'), may hold values from -0.5 to 0.5
- mix_bias: float32 [8, 128], P('tp'), may hold values from 0.1 to 1.9
- back_weight: bfloat16 [1024, 2048], P('fs', 'tp'), may hold values from -0.1875 to 0.1875
- mid_gain: float32 [2048], replicated, may hold values from 0.1 to 1.9
- hidden_weight: bfloat16 [2048, 8192], P('fs', 'tp'), may hold values from -0.125 to 0.125
- down_weight: bfloat16 [8192, 2048], P('tp', 'fs'), may hold values from -0.0625 to 0.0625
- last_gain: float32 [2048], replicated, may hold values from 0.1 to 1.9
Outputs:
- layer_out: bfloat16 [4096, 2048], P(('rep', 'fs'), 'tp')
All inputs are finite; a program needn't handle non-finite values.
Results may differ from a plain program's by a relative error of at most 0.015.
Values may be sent and summed in bfloat16 or wider, within the bound.
A program may use at most 128 MiB of HBM per device.

v0:
```python
import jax
import jax.numpy as jnp
from jax import lax
from jax.sharding import PartitionSpec as P

EPS = 1e-06


def normalize(values, gain, total, width):
    return values * lax.rsqrt(total / width + EPS) * gain


def on_device(
    tokens,
    first_gain,
    up_weight,
    value_weight,
    value_gain,
    mix_weight,
    mix_bias,
    back_weight,
    mid_gain,
    hidden_weight,
    down_weight,
    last_gain,
):
    col_count = tokens.shape[1]
    row_count = tokens.shape[0]
    width = col_count * lax.axis_size("tp")
    offset = lax.axis_index("tp") * col_count
    inputs = tokens.astype(jnp.float32)
    whole_in = lax.all_gather(tokens, "tp", axis=1, tiled=True).astype(jnp.float32)
    normed = normalize(
        whole_in, first_gain, jnp.sum(whole_in * whole_in, axis=1, keepdims=True), width
    ).astype(jnp.bfloat16)
    gw_dev = up_weight.shape[1]
    block = normed
    up_pre = jnp.dot(
        block,
        lax.all_gather(up_weight, "fs", axis=0, tiled=True),
        preferred_element_type=jnp.float32,
    )
    value_pre = jnp.dot(
        block,
        lax.all_gather(value_weight, "fs", axis=0, tiled=True),
        preferred_element_type=jnp.float32,
    )
    up_part = jax.nn.gelu(up_pre, approximate=False).astype(jnp.bfloat16)
    value_act = jax.nn.gelu(value_pre, approximate=False)
    value_total = lax.psum(jnp.sum(value_act * value_act, axis=1, keepdims=True), "tp")
    value_normed = normalize(
        value_act, value_gain, value_total, gw_dev * lax.axis_size("tp")
    ).astype(jnp.bfloat16)
    group_dev = mix_weight.shape[0]
    span = mix_weight.shape[1]
    causal = jnp.tril(jnp.ones((span, span), dtype=bool))
    masked = jnp.where(causal[None], mix_weight, jnp.zeros_like(mix_weight))
    blocks = value_normed.reshape(row_count // span, span, group_dev, gw_dev // group_dev)
    mixed = (
        jnp.einsum("gts,nsgc->ntgc", masked, blocks, preferred_element_type=jnp.float32)
        + mix_bias.T[None, :, :, None]
    )
    gated = (up_part.astype(jnp.float32) * mixed.reshape(row_count, gw_dev)).astype(jnp.bfloat16)
    gated_all = lax.all_gather(gated, "tp", axis=1, tiled=True)
    block = gated_all
    back = jnp.dot(
        block,
        lax.all_gather(back_weight, "fs", axis=0, tiled=True),
        preferred_element_type=jnp.float32,
    )
    stream = (inputs + back).astype(jnp.bfloat16)
    stream_f = stream.astype(jnp.float32)
    whole_mid = lax.all_gather(stream, "tp", axis=1, tiled=True).astype(jnp.float32)
    mid_normed = normalize(
        whole_mid, mid_gain, jnp.sum(whole_mid * whole_mid, axis=1, keepdims=True), width
    ).astype(jnp.bfloat16)
    block = mid_normed
    hidden_pre = jnp.dot(
        block,
        lax.all_gather(hidden_weight, "fs", axis=0, tiled=True),
        preferred_element_type=jnp.float32,
    )
    hidden = jnp.square(jax.nn.relu(hidden_pre)).astype(jnp.bfloat16)
    partial_terms = jnp.dot(
        hidden,
        lax.all_gather(down_weight, "fs", axis=1, tiled=True),
        preferred_element_type=jnp.float32,
    )
    channel_out = lax.psum_scatter(
        partial_terms.astype(jnp.bfloat16), "tp", scatter_dimension=1, tiled=True
    ).astype(jnp.float32)
    final = stream_f + channel_out
    final_total = lax.psum(jnp.sum(final * final, axis=1, keepdims=True), "tp")
    return normalize(
        final, lax.dynamic_slice_in_dim(last_gain, offset, col_count), final_total, width
    ).astype(jnp.bfloat16)


def solution(mesh):
    return jax.shard_map(
        on_device,
        mesh=mesh,
        in_specs=(
            P(("rep", "fs"), "tp"),
            P(),
            P("fs", "tp"),
            P("fs", "tp"),
            P("tp"),
            P("tp", None, None),
            P("tp", None),
            P("fs", "tp"),
            P(),
            P("fs", "tp"),
            P("tp", "fs"),
            P(),
        ),
        out_specs=P(("rep", "fs"), "tp"),
        check_vma=False,
    )
```

profile of v0, /device:TPU:0, one launch (start us, length us, event | category | flops | bytes accessed | tf_op | source)
XLA Modules:
  0.0 677.3 jit_solution(15823394107701373287)
XLA Ops:
  6.5 0.7 all-gather.8.cloned.1.call-update
  7.3 0.7 all-gather.12.cloned.1.call-update
  8.1 0.7 all-gather.10.cloned.1.call-update
  8.8 0.5 all-gather.14.cloned.1.call-update
  9.4 11.3 %all-gather.8.cloned.1.call-done = bf16[256,2048]{1,0:T(8,128)(2,1)} async-done(((bf16[256,1024]{1,0:T(8,128)(2,1)}), bf16[256,2048]{1,0:T(8,128)(2,1)}) %all-gather.8.cloned.1.call-update) | async-done | bytes 1048592 | tf_op jit(solution)/shard_map/all_gather | solution.py:32
  20.7 1.5 fusion.2
  22.2 50.9 %all-gather.12.cloned.1.call-done = bf16[2048,512]{1,0:T(8,128)(2,1)} async-done(((bf16[256,512]{1,0:T(8,128)(2,1)}), bf16[2048,512]{1,0:T(8,128)(2,1)}) %all-gather.12.cloned.1.call-update) | async-done | bytes 2097168 | tf_op jit(solution)/shard_map/all_gather | solution.py:45
  73.1 3.8 multiply_reduce_fusion.1
  76.9 2.6 psum.14
  80.3 42.6 %all-gather.10.cloned.1.call-done = bf16[2048,512]{1,0:T(8,128)(2,1)} async-done(((bf16[256,512]{1,0:T(8,128)(2,1)}), bf16[2048,512]{1,0:T(8,128)(2,1)}) %all-gather.10.cloned.1.call-update) | async-done | bytes 2097168 | tf_op jit(solution)/shard_map/all_gather | solution.py:40
  122.9 3.5 fusion.20
  126.4 2.2 all_gather.27
  128.5 43.9 %all-gather.14.cloned.1.call-done = bf16[1024,1024]{1,0:T(8,128)(2,1)} async-done(((bf16[128,1024]{1,0:T(8,128)(2,1)}), bf16[1024,1024]{1,0:T(8,128)(2,1)}) %all-gather.14.cloned.1.call-update) | async-done | bytes 2097168 | tf_op jit(solution)/shard_map/all_gather | solution.py:68
  172.5 3.1 fusion.8
  176.3 0.7 all-gather.20.cloned.1.call-update
  177.0 6.3 all-gather.16.cloned.1.call-done
  183.3 1.5 fusion.5
  184.9 228.9 %all-gather.18.cloned.1.call-done = bf16[2048,4096]{1,0:T(8,128)(2,1)} async-done(((bf16[256,4096]{1,0:T(8,128)(2,1)}), bf16[2048,4096]{1,0:T(8,128)(2,1)}) %all-gather.18.cloned.1.call-update) | async-done | bytes 16777232 | tf_op jit(solution)/shard_map/all_gather | solution.py:80
  413.8 227.6 %all-gather.20.cloned.1.call-done = bf16[4096,2048]{1,0:T(8,128)(2,1)} async-done(((bf16[4096,256]{1,0:T(8,128)(2,1)}), bf16[4096,2048]{1,0:T(8,128)(2,1)}) %all-gather.20.cloned.1.call-update) | async-done | bytes 16777232 | tf_op jit(solution)/shard_map/all_gather | solution.py:86
  641.4 16.5 %convolution_convert_fusion = bf16[256,2048]{1,0:T(8,128)(2,1)} fusion(bf16[4096,2048]{1,0:T(8,128)(2,1)} %all-gather.20.cloned.1.call-done, bf16[2048,4096]{1,0:T(8,128)(2,1)} %all-gather.18.cloned.1.call-done, bf16[256,2048]{1,0:T(8,128)(2,1)} %all-gather.16.cloned.1.call-done, f32[2048]{0:T(1024)S(1)} %copy-done.8, f32[256]{0:T(256)S(1)} %add_rsqrt_fusion.1), kind=kOutput, calls=%fused_computation.7 | convolution fusion | flops 8595701760 | bytes 35660800 | tf_op jit(solution)/shard_map/dot_general | solution.py:84
  658.0 6.7 reduce-scatter.2.cloned.1.call-done
  664.7 1.3 multiply_reduce_fusion
  666.0 2.5 psum.15
  668.4 2.0 multiply_convert_fusion
  (39 shorter events, 1.6 us)
Async XLA Ops:
  6.5 66.5 %copy-start.7 = (f32[2048]{0:T(1024)S(1)}, f32[2048]{0:T(1024)}, u32[]{:S(2)}) copy-start(f32[2048]{0:T(1024)} %param.13) | copy-start | bytes 24580
  6.5 14.1 %all-gather.8.cloned.1.call-start = ((), (), s32[]{:S(2)}) async-start(), calls=%async_computation.1 | async-start | bytes 1572864 | tf_op jit(solution)/shard_map/all_gather | solution.py:32
  7.3 65.8 %all-gather.12.cloned.1.call-start = ((), (), s32[]{:S(2)}) async-start(), calls=%async_computation.3 | async-start | bytes 2359296 | tf_op jit(solution)/shard_map/all_gather | solution.py:45
  8.0 114.9 %all-gather.10.cloned.1.call-start = ((), (), s32[]{:S(2)}) async-start(), calls=%async_computation.2 | async-start | bytes 2359296 | tf_op jit(solution)/shard_map/all_gather | solution.py:40
  8.7 163.8 %all-gather.14.cloned.1.call-start = ((), (), s32[]{:S(2)}) async-start(), calls=%async_computation.4 | async-start | bytes 2359296 | tf_op jit(solution)/shard_map/all_gather | solution.py:68
  9.3 174.0 %all-gather.16.cloned.1.call-start = ((), (), s32[]{:S(2)}) async-start(), calls=%async_computation.5 | async-start | bytes 1572864 | tf_op jit(solution)/shard_map/all_gather | solution.py:73
  22.2 57.4 %copy-start.4 = (f32[512]{0:T(512)S(1)}, f32[512]{0:T(512)}, u32[]{:S(2)}) copy-start(f32[512]{0:T(512)} %param.16) | copy-start | bytes 6148
  22.2 57.6 %copy-start.3 = (bf16[4,128,128]{2,1,0:T(8,128)(2,1)S(1)}, bf16[4,128,128]{2,1,0:T(8,128)(2,1)}, u32[]{:S(2)}) copy-start(bf16[4,128,128]{2,1,0:T(8,128)(2,1)} %param.17) | copy-start | bytes 393220
  22.2 57.6 %copy-start.5 = (f32[4,128]{1,0:T(4,128)S(1)}, f32[4,128]{1,0:T(4,128)}, u32[]{:S(2)}) copy-start(f32[4,128]{1,0:T(4,128)} %param.18) | copy-start | bytes 6148
  76.9 45.9 %copy-start.1 = (bf16[256,2048]{1,0:T(8,128)(2,1)S(1)}, bf16[256,2048]{1,0:T(8,128)(2,1)}, u32[]{:S(2)}) copy-start(bf16[256,2048]{1,0:T(8,128)(2,1)} %all-gather.8.cloned.1.call-done) | copy-start | bytes 3145732
  122.9 49.6 %copy-start.2 = (bf16[256,1024]{1,0:T(8,128)(2,1)S(1)}, bf16[256,1024]{1,0:T(8,128)(2,1)}, u32[]{:S(2)}) copy-start(bf16[256,1024]{1,0:T(8,128)(2,1)} %param.12) | copy-start | bytes 1572868
  175.6 238.2 %all-gather.18.cloned.1.call-start = ((), (), s32[]{:S(2)}) async-start(), calls=%async_computation.6 | async-start | bytes 18874368 | tf_op jit(solution)/shard_map/all_gather | solution.py:80
  176.2 465.2 %copy-start.8 = (f32[2048]{0:T(1024)S(1)}, f32[2048]{0:T(1024)}, u32[]{:S(2)}) copy-start(f32[2048]{0:T(1024)} %param.20) | copy-start | bytes 24580
  176.2 465.2 %all-gather.20.cloned.1.call-start = ((), (), s32[]{:S(2)}) async-start(), calls=%async_computation.7 | async-start | bytes 18874368 | tf_op jit(solution)/shard_map/all_gather | solution.py:86
  177.0 487.7 %reduce-scatter.2.cloned.1.call-start = ((), (), s32[]{:S(2)}) async-start(), calls=%async_computation.8 | async-start | bytes 1572864 | tf_op jit(solution)/shard_map/reduce_scatter | solution.py:89
  184.9 473.1 %copy-start.6 = (f32[2048]{0:T(1024)S(1)}, f32[2048]{0:T(1024)}, u32[]{:S(2)}) copy-start(f32[2048]{0:T(1024)} %param.23) | copy-start | bytes 24580
  184.9 479.8 %copy-start = (bf16[256,1024]{1,0:T(8,128)(2,1)S(1)}, bf16[256,1024]{1,0:T(8,128)(2,1)}, u32[]{:S(2)}) copy-start(bf16[256,1024]{1,0:T(8,128)(2,1)} %fusion.8) | copy-start | bytes 1572868
Sparse Core Ops, SparseCore 0:
  8.9 11.7 all-gather.7
  22.8 50.2 all-gather.11
  75.2 47.6 all-gather.9
  124.8 47.6 all-gather.13
  175.7 7.5 all-gather.15
  185.3 228.4 all-gather.17
  415.9 225.4 all-gather.19
  658.0 6.5 reduce-scatter.1
where the time goes:
time: 678 us; the launch traced here: 677 us
  waiting for transfers between devices  622 us (92%)
  matrix products  27.3 us (4%)
  between operations  13.6 us (2%)
  blocking collectives  7.25 us (1%)
    all_gather x1, waiting for transfers between devices, on_device(): lax.all_gather(hidden_weight, 'fs', axis=0, tiled=True)  229 us
    all_gather x1, waiting for transfers between devices, on_device(): lax.all_gather(down_weight, 'fs', axis=1, tiled=True)  228 us
    all_gather x1, waiting for transfers between devices, on_device(): lax.all_gather(value_weight, 'fs', axis=0, tiled=True)  50.9 us
    all_gather x1, waiting for transfers between devices, on_device(): lax.all_gather(back_weight, 'fs', axis=0, tiled=True)  43.9 us
    all_gather x1, waiting for transfers between devices, on_device(): lax.all_gather(up_weight, 'fs', axis=0, tiled=True)  42.6 us
    dot_general x1, matrix products, on_device(): jnp.dot(hidden, lax.all_gather(down_weight, 'fs', axis=1, tiled=True), pr...  16.5 us
  transfers between devices with their start and end apart: 8, of which 8 were waited for; matrix products, arithmetic and copies ran while one was open for 2% of the time, Pallas kernels for 0%

commit v1 on v0

--- a/solution.py
+++ b/solution.py
@@ -1,9 +1,475 @@
+import functools
+
 import jax
 import jax.numpy as jnp
 from jax import lax
+from jax.experimental import pallas as pl
+from jax.experimental.pallas import tpu as pltpu
 from jax.sharding import PartitionSpec as P
 
 EPS = 1e-06
+MESH = pl.DeviceIdType.MESH
+BF = jnp.bfloat16
+F32 = jnp.float32
+ALPHA = (
+    0.00022905065861350646,
+    0.0034082910107109506,
+    0.050955695062380861,
+    0.18520832239976145,
+    1.128379143519084,
+)
+BETA = (
+    -1.1791602954361697e-7,
+    0.000023547966471313185,
+    0.0010179625278914885,
+    0.014070470171167667,
+    0.11098505178285362,
+    0.49746925110067538,
+    1.0,
+)
+
+
+def horner(x, coefs):
+    acc = jnp.full_like(x, coefs[0])
+    for c in coefs[1:]:
+        acc = acc * x + c
+    return acc
+
+
+def gelu(x):
+    z = jnp.clip(x * 0.7071067811865476, -3.7439211627767994, 3.7439211627767994)
+    z2 = z * z
+    return 0.5 * x * (1.0 + z * horner(z2, ALPHA) / horner(z2, BETA))
+
+
+def kernel(
+    dims,
+    tok,
+    g1,
+    up,
+    val,
+    vg,
+    mw,
+    mb,
+    back,
+    g2,
+    hid,
+    down,
+    g3,
+    out,
+    xbuf,
+    nbuf,
+    upw,
+    vaw,
+    bw,
+    hw,
+    dw,
+    vgb,
+    mwb,
+    mbb,
+    upact,
+    vact,
+    gated,
+    sbuf,
+    ag,
+    part,
+    rsr,
+    rss,
+    ybuf,
+    yin,
+    tok_s,
+    ring_s,
+    rlast_s,
+    pw_s,
+    a2_s,
+    x_s,
+    hd_s,
+    ag_s,
+    rs_s,
+    y_s,
+):
+    n, half_rows, cd, span = dims
+    dk, gwd = up.shape
+    bk = back.shape[0]
+    fu = hw.shape[4]
+    dcol = down.shape[1]
+    width = 2 * cd
+    gw = 2 * gwd
+    groups = mw.shape[0]
+    gc = gwd // groups
+    r, f, t = lax.axis_index("rep"), lax.axis_index("fs"), lax.axis_index("tp")
+    zn = n // 2
+    z, y = f // 2, f % 2
+    pos = z * (1 - y) + (n - 1 - z) * y
+
+    def fs_of(p):
+        hi = p // zn
+        return (2 * p) * (1 - hi) + (2 * (n - 1 - p) + 1) * hi
+
+    def ring(p):
+        return lax.rem(p + 2 * n, n)
+
+    partner = (r, f, 1 - t)
+    xpeer = (1 - r, f, t)
+    nbr = [(r, fs_of(ring(pos + 1)), t), (r, fs_of(ring(pos - 1)), t)]
+    sgn = (1, -1)
+
+    def hops(d, c):
+        return n // 2 if d == c else n // 2 - 1
+
+    sent = []
+
+    def send(src, dst, sems, dev):
+        ss, rs = sems
+        cp = pltpu.make_async_remote_copy(
+            src_ref=src, dst_ref=dst, send_sem=ss, recv_sem=rs, device_id=dev, device_id_type=MESH
+        )
+        cp.start()
+        sent.append(cp)
+
+    def landed(ref, sems, dev):
+        ss, rs = sems
+        pltpu.make_async_remote_copy(
+            src_ref=ref, dst_ref=ref, send_sem=ss, recv_sem=rs, device_id=dev, device_id_type=MESH
+        ).wait_recv()
+
+    barrier = pltpu.get_barrier_semaphore()
+    for k in range(1, n):
+        pl.semaphore_signal(
+            barrier, inc=1, device_id=(r, lax.rem(f + k, n), t), device_id_type=MESH
+        )
+    pl.semaphore_signal(barrier, inc=1, device_id=partner, device_id_type=MESH)
+    pl.semaphore_signal(barrier, inc=1, device_id=xpeer, device_id_type=MESH)
+    pl.semaphore_wait(barrier, n + 1)
+
+    def sem2(s, *i):
+        return s.at[(0,) + i], s.at[(1,) + i]
+
+    bh = bk // 2
+
+    def slots(q, c, tt):
+        fq = fs_of(q)
+        w = upw if c == 0 else vaw
+        rows = pl.ds(pl.multiple_of(fq * bk + c * bh, bh), bh)
+        return w.at[tt, fq], bw.at[tt, rows, :]
+
+    def own(c):
+        return (up, val)[c], back.at[pl.ds(c * bh, bh), :]
+
+    def ring_send(s, d, c):
+        q = ring(pos - sgn[d] * s)
+        dst = slots(q, c, t)
+        src = own(c) if s == 0 else dst
+        for i in range(2):
+            send(src[i], dst[i], sem2(ring_s, d, c, s, i), nbr[d])
+
+    for d in range(2):
+        for c in range(2):
+            ring_send(0, d, c)
+
+    rows_own = pl.ds(pl.multiple_of(t * half_rows, half_rows), half_rows)
+    rows_oth = pl.ds(pl.multiple_of((1 - t) * half_rows, half_rows), half_rows)
+    send(tok.at[rows_oth, :], xbuf.at[t], sem2(tok_s, 0), partner)
+    send(vg, vgb.at[t], sem2(tok_s, 1), partner)
+    send(mw, mwb.at[t], sem2(tok_s, 2), partner)
+    send(mb, mbb.at[t], sem2(tok_s, 3), partner)
+    for c in range(2):
+        dst = slots(pos, c, t)
+        src = own(c)
+        for i in range(2):
+            send(src[i], dst[i], sem2(pw_s, 0, 0, c, i), partner)
+
+    hr, dr = hid.shape[0] // 2, fu // 2
+
+    def hpiece(tt, ff, rr):
+        return hw.at[tt, ff, rr]
+
+    def dpiece(tt, ff, rr):
+        return dw.at[tt, rr, :, pl.ds(pl.multiple_of(ff * dcol, dcol), dcol)]
+
+    def a2a_send(k):
+        g = lax.rem(f + k, n)
+        dev = (r, g, t)
+        send(
+            hid.at[
+                pl.ds(pl.multiple_of(r * hr, hr), hr), pl.ds(pl.multiple_of(g * fu, fu), fu)
+            ],
+            hpiece(t, f, r),
+            sem2(a2_s, k, 0),
+            dev,
+        )
+        send(
+            down.at[pl.ds(pl.multiple_of(g * fu + r * dr, dr), dr), :],
+            dpiece(t, f, r),
+            sem2(a2_s, k, 1),
+            dev,
+        )
+
+    for c in range(2):
+        w = (upw, vaw)[c]
+        w[t, f] = (up, val)[c][...]
+    bw[t, pl.ds(pl.multiple_of(f * bk, bk), bk), :] = back[...]
+    own_cols = pl.ds(pl.multiple_of(f * fu, fu), fu)
+    for rr in range(2):
+        hw[t, f, rr] = hid[rr * hr : (rr + 1) * hr, own_cols]
+        dw[t, rr, :, pl.ds(pl.multiple_of(f * dcol, dcol), dcol)] = down[
+            pl.ds(pl.multiple_of(f * fu + rr * dr, dr), dr), :
+        ]
+    xbuf[t] = tok[rows_own, :]
+    vgb[t] = vg[...]
+    mwb[t] = mw[...]
+    mbb[t] = mb[...]
+
+    steps = n // 2
+    ks = list(range(1, n))
+    for s in range(1, steps):
+        for k in ks[: -(-(n - 1) // (steps - 1))]:
+            a2a_send(k)
+        ks = ks[-(-(n - 1) // (steps - 1)) :]
+        for d in range(2):
+            for c in range(2):
+                q = ring(pos - sgn[d] * s)
+                land = slots(q, c, t)
+                for i in range(2):
+                    landed(land[i], sem2(ring_s, d, c, s - 1, i), nbr[d])
+                if s < hops(d, c):
+                    ring_send(s, d, c)
+                for i in range(2):
+                    send(land[i], land[i], sem2(pw_s, s, d, c, i), partner)
+        if s == 1:
+            for i, ref in enumerate((xbuf.at[1 - t], vgb.at[1 - t], mwb.at[1 - t], mbb.at[1 - t])):
+                landed(ref, sem2(tok_s, i), partner)
+            xs = [xbuf[i].astype(F32) for i in range(2)]
+            tot = sum(jnp.sum(v * v, axis=1, keepdims=True) for v in xs)
+            sc = lax.rsqrt(tot / width + EPS)
+            for i in range(2):
+                cols = slice(i * cd, (i + 1) * cd)
+                nbuf[:, cols] = (xs[i] * sc * g1[:, cols]).astype(BF)
+    for d in range(2):
+        q = ring(pos - sgn[d] * steps)
+        land = slots(q, d, t)
+        for i in range(2):
+            landed(land[i], sem2(ring_s, d, d, steps - 1, i), nbr[d])
+            send(land[i], land[i], sem2(pw_s, steps, d, d, i), partner)
+    def relay(k):
+        g = lax.rem(f - k + n, n)
+        hp, dp = hpiece(t, g, r), dpiece(t, g, r)
+        for i, p in enumerate((hp, dp)):
+            landed(p, sem2(a2_s, k, i), (r, g, t))
+            send(p, p, sem2(x_s, k, i), xpeer)
+            send(p, p, sem2(hd_s, k, i, 0), partner)
+
+    for c in range(2):
+        for i in range(2):
+            landed(slots(pos, c, 1 - t)[i], sem2(pw_s, 0, 0, c, i), partner)
+    for s in range(1, steps + 1):
+        for d in range(2):
+            for c in range(2):
+                if s <= hops(d, c):
+                    q = ring(pos - sgn[d] * s)
+                    for i in range(2):
+                        landed(slots(q, c, 1 - t)[i], sem2(pw_s, s, d, c, i), partner)
+    for rr in range(2):
+        send(hpiece(t, f, rr), hpiece(t, f, rr), sem2(hd_s, 0, 0, rr), partner)
+        send(dpiece(t, f, rr), dpiece(t, f, rr), sem2(hd_s, 0, 1, rr), partner)
+    for k in range(1, n // 2):
+        relay(k)
+
+    @pl.loop(0, 2)
+    def _(tt):
+        a = jnp.dot(nbuf[...], upw[tt].reshape(width, gwd), preferred_element_type=F32)
+        upact[tt] = gelu(a).astype(BF)
+        b = jnp.dot(nbuf[...], vaw[tt].reshape(width, gwd), preferred_element_type=F32)
+        vact[tt] = gelu(b)
+
+    vs = [vact[i] for i in range(2)]
+    tot = sum(jnp.sum(v * v, axis=1, keepdims=True) for v in vs)
+    vsc = lax.rsqrt(tot / gw + EPS)
+    row_i = lax.broadcasted_iota(jnp.int32, (span, span), 0)
+    col_i = lax.broadcasted_iota(jnp.int32, (span, span), 1)
+    for tt in range(2):
+        vn = (vs[tt] * vsc * vgb[tt]).astype(BF)
+        for g in range(groups):
+            m = mwb[tt, g]
+            m = jnp.where(col_i <= row_i, m, jnp.zeros_like(m))
+            bias = jnp.broadcast_to(mbb[tt, g : g + 1, :], (span, span))
+            bias = jnp.sum(jnp.where(col_i == row_i, bias, 0.0), axis=1, keepdims=True)
+            cs = slice(g * gc, (g + 1) * gc)
+            for b in range(half_rows // span):
+                rs_ = slice(b * span, (b + 1) * span)
+                mx = jnp.dot(m, vn[rs_, cs], preferred_element_type=F32) + bias
+                gated[rs_, tt * gwd + g * gc : tt * gwd + (g + 1) * gc] = (
+                    upact[tt, rs_, cs].astype(F32) * mx
+                ).astype(BF)
+
+    @pl.loop(0, 2)
+    def _(tt):
+        acc = jnp.dot(gated[...], bw[tt], preferred_element_type=F32)
+        sbuf[tt] = (xbuf[tt].astype(F32) + acc).astype(BF)
+
+    ss_ = [sbuf[i].astype(F32) for i in range(2)]
+    tot = sum(jnp.sum(v * v, axis=1, keepdims=True) for v in ss_)
+    sc = lax.rsqrt(tot / width + EPS)
+    for i in range(2):
+        ag[pos, i] = (ss_[i] * sc * g2[:, i * cd : (i + 1) * cd]).astype(BF)
+
+    def ag_send(s, d, c):
+        q = ring(pos - sgn[d] * s)
+        send(ag.at[q, c], ag.at[q, c], sem2(ag_s, d, c, s), nbr[d])
+
+    for d in range(2):
+        for c in range(2):
+            ag_send(0, d, c)
+
+    for k in range(n // 2, n):
+        relay(k)
+    for k in range(1, n):
+        g = lax.rem(f - k + n, n)
+        for i, p in enumerate((hpiece(t, g, 1 - r), dpiece(t, g, 1 - r))):
+            landed(p, sem2(x_s, k, i), xpeer)
+            send(p, p, sem2(hd_s, k, i, 1), partner)
+    for rr in range(2):
+        landed(hpiece(1 - t, f, rr), sem2(hd_s, 0, 0, rr), partner)
+        landed(dpiece(1 - t, f, rr), sem2(hd_s, 0, 1, rr), partner)
+    for k in range(1, n):
+        g = lax.rem(f - k + n, n)
+        for j, rr in enumerate((r, 1 - r)):
+            landed(hpiece(1 - t, g, rr), sem2(hd_s, k, 0, j), partner)
+            landed(dpiece(1 - t, g, rr), sem2(hd_s, k, 1, j), partner)
+
+    def mixer(q):
+        a = jnp.concatenate([ag[q, 0], ag[q, 1]], axis=1)
+        hs = []
+        for tt in range(2):
+            p = jnp.dot(a, hw[tt].reshape(width, fu), preferred_element_type=F32)
+            p = jnp.maximum(p, 0.0)
+            hs.append((p * p).astype(BF))
+        h = jnp.concatenate(hs, axis=1)
+        w = dw[...].reshape(2 * fu, width)
+        for c in range(2):
+            part[q, c] = jnp.dot(h, w[:, c * cd : (c + 1) * cd], preferred_element_type=F32)
+
+    for s in range(1, steps + 1):
+        for d in range(2):
+            for c in range(2):
+                if s <= hops(d, c):
+                    q = ring(pos - sgn[d] * s)
+                    landed(ag.at[q, c], sem2(ag_s, d, c, s - 1), nbr[d])
+                    if s < hops(d, c):
+                        ag_send(s, d, c)
+        if s == 1:
+
+            @pl.loop(0, 3)
+            def _(j):
+                mixer(ring(pos + j - 1))
+        elif s < steps:
+
+            @pl.loop(0, 2)
+            def _(j):
+                mixer(ring(pos + s - 2 * s * j))
+        else:
+            mixer(ring(pos + s))
+
+    for s in range(steps):
+        for d in range(2):
+            for c in range(2):
+                h = hops(d, c)
+                if s < h:
+                    dest = ring(pos + sgn[d] * (h - s))
+                    v = part[dest, c]
+                    if s > 0:
+                        landed(rsr.at[d, c, s - 1], sem2(rs_s, d, c, s - 1), nbr[d])
+                        v = v + rsr[d, c, s - 1].astype(F32)
+                    rss[d, c, s] = v.astype(BF)
+                    send(rss.at[d, c, s], rsr.at[d, c, s], sem2(rs_s, d, c, s), nbr[d])
+    fin = []
+    for c in range(2):
+        v = part[pos, c]
+        for d in range(2):
+            h = hops(d, c)
+            landed(rsr.at[d, c, h - 1], sem2(rs_s, d, c, h - 1), nbr[d])
+            v = v + rsr[d, c, h - 1].astype(F32)
+        fin.append(sbuf[c].astype(F32) + v)
+    tot = sum(jnp.sum(v * v, axis=1, keepdims=True) for v in fin)
+    sc = lax.rsqrt(tot / width + EPS)
+    for c in range(2):
+        ybuf[c] = (fin[c] * sc * g3[:, c * cd : (c + 1) * cd]).astype(BF)
+    send(ybuf.at[1 - t], yin, sem2(y_s, 0), partner)
+    out[rows_own, :] = ybuf[t]
+    landed(yin, sem2(y_s, 0), partner)
+    out[rows_oth, :] = yin[...]
+    for cp in sent:
+        cp.wait_send()
+
+
+def fused(mesh, *args):
+    tok, g1, up, val, vg, mw, mb, back, g2, hid, down, g3 = args
+    n = mesh.shape["fs"]
+    rows, cd = tok.shape
+    hrows = rows // 2
+    span = mw.shape[1]
+    dk, gwd = up.shape
+    bk = back.shape[0]
+    fu = hid.shape[1] // n
+    steps = n // 2
+    dims = (n, hrows, cd, span)
+    v = pltpu.VMEM
+    dma = pltpu.SemaphoreType.DMA
+    scratch = [
+        v((2, hrows, cd), BF),
+        v((hrows, 2 * cd), BF),
+        v((2, n, dk, gwd), BF),
+        v((2, n, dk, gwd), BF),
+        v((2, n * bk, cd), BF),
+        v((2, n, 2, dk // 2, fu), BF),
+        v((2, 2, fu // 2, 2 * cd), BF),
+        v((2, 1, gwd), F32),
+        v((2,) + mw.shape, BF),
+        v((2,) + mb.shape, F32),
+        v((2, hrows, gwd), BF),
+        v((2, hrows, gwd), F32),
+        v((hrows, 2 * gwd), BF),
+        v((2, hrows, cd), BF),
+        v((n, 2, hrows, cd), BF),
+        v((n, 2, hrows, cd), F32),
+        v((2, 2, steps, hrows, cd), BF),
+        v((2, 2, steps, hrows, cd), BF),
+        v((2, hrows, cd), BF),
+        v((hrows, cd), BF),
+        dma((2, 4)),
+        dma((2, 2, 2, steps, 2)),
+        dma((1,)),
+        dma((2, steps + 1, 2, 2, 2)),
+        dma((2, n, 2)),
+        dma((2, n, 2)),
+        dma((2, n, 2, 2)),
+        dma((2, 2, 2, steps)),
+        dma((2, 2, 2, steps)),
+        dma((2, 1)),
+    ]
+    return pl.pallas_call(
+        functools.partial(kernel, dims),
+        out_shape=jax.ShapeDtypeStruct((rows, cd), BF),
+        in_specs=[pl.BlockSpec(memory_space=pltpu.VMEM)] * 12,
+        out_specs=pl.BlockSpec(memory_space=pltpu.VMEM),
+        scratch_shapes=scratch,
+        compiler_params=pltpu.CompilerParams(
+            collective_id=0, has_side_effects=True, vmem_limit_bytes=62 * 1024 * 1024
+        ),
+    )(
+        tok,
+        g1.reshape(1, -1),
+        up,
+        val,
+        vg.reshape(1, -1),
+        mw,
+        mb,
+        back,
+        g2.reshape(1, -1),
+        hid,
+        down,
+        g3.reshape(1, -1),
+    )
 
 
 def normalize(values, gain, total, width):
@@ -96,9 +562,28 @@
     ).astype(jnp.bfloat16)
 
 
+def fits(mesh, args):
+    tok, _, up, _, _, mw, _, back, _, hid, down, _ = args
+    n = mesh.shape["fs"]
+    rows, cd = tok.shape
+    hrows = rows // 2
+    fu = hid.shape[1] // n
+    if mesh.shape["rep"] != 2 or mesh.shape["tp"] != 2 or n % 2 or n < 4:
+        return False
+    if hrows % mw.shape[1] or fu % 256 or down.shape[1] % 128 or back.shape[0] % 32:
+        return False
+    held = 2 * (up.size * 2 + back.size + hid.size + down.size)
+    held += 4 * n * (up.size * 2 + back.size) + 4 * (hid.size + down.size)
+    held += n * 2 * hrows * cd * 6 + 8 * n * hrows * cd
+    return held < 52 * 2**20
+
+
 def solution(mesh):
+    def on_any(*args):
+        return fused(mesh, *args) if fits(mesh, args) else on_device(*args)
+
     return jax.shard_map(
-        on_device,
+        on_any,
         mesh=mesh,
         in_specs=(
             P(("rep", "fs"), "tp"),

time: 678 us -> 240 us (0.35)
  waiting for transfers between devices: 622 us -> 0 us
  Pallas kernels: 0 us -> 237 us
  matrix products: 27.3 us -> 0 us
  between operations: 13.6 us -> 0.01 us
  blocking collectives: 7.25 us -> 0 us
    all_gather x7 -> x0, waiting for transfers between devices: 611 us -> none  [the longest x1 229 us: on_device(): lax.all_gather(hidden_weight, 'fs', axis=0, tiled=True)]
    pallas_call x0 -> x1, Pallas kernels: none -> 237 us  [fused(): pl.pallas_call(functools.partial(kernel, dims), out_shape=jax.ShapeDtypeS...]
    dot_general x5 -> x0, matrix products: 27.3 us -> none  [the longest x1 16.5 us: on_device(): jnp.dot(hidden, lax.all_gather(down_weight, 'fs', axis=1, tiled=True), pr...]
  transfers between devices with their start and end apart: 8 -> 0, of which waited for: 8 -> 0; matrix products, arithmetic and copies ran while one was open for 2% -> 0% of each run, Pallas kernels for 0% -> 0%
where the time goes in v1:
time: 240 us; the launch traced here: 239 us
  Pallas kernels  237 us (99%)
    pallas_call x1, Pallas kernels, fused(): pl.pallas_call(functools.partial(kernel, dims), out_shape=jax.ShapeDtypeS...  237 us

profile of v1, /device:TPU:0, one launch (start us, length us, event | category | flops | bytes accessed | tf_op | source)
XLA Modules:
  0.0 239.3 jit_solution(12316194131245472845)
XLA Ops:
  0.0 237.4 %shard_map.118 = bf16[256,1024]{1,0:T(8,128)(2,1)} custom-call(bf16[256,1024]{1,0:T(8,128)(2,1)} %tok.1, f32[1,2048]{1,0:T(1,128)} %bitcast.4, bf16[256,512]{1,0:T(8,128)(2,1)} %up.1, bf16[256,512]{1,0:T(8,128)(2,1)} %val.1, f32[1,512]{1,0:T(1,128)} %bitcast.7, bf16[4,128,128]{2,1,0:T(8,128)(2,1)} %mw.1, f32[4,128]{1,0:T(4,128)} %mb.1, ...), custom_call_target="tpu_custom_call" | custom-call | tf_op jit(solution)/shard_map/pallas_call | solution.py:450
  237.4 1.9 copy.14

commit v2 on v1

--- a/solution.py
+++ b/solution.py
@@ -67,8 +67,9 @@
     vgb,
     mwb,
     mbb,
+    upacc,
+    vact,
     upact,
-    vact,
     gated,
     sbuf,
     ag,
@@ -79,8 +80,9 @@
     yin,
     tok_s,
     ring_s,
-    rlast_s,
+    xr_s,
     pw_s,
+    px_s,
     a2_s,
     x_s,
     hd_s,
@@ -146,26 +148,38 @@
         return s.at[(0,) + i], s.at[(1,) + i]
 
     bh = bk // 2
-
-    def slots(q, c, tt):
+    bq = bh // 2
+    ub = 5 * dk // 256 * 16
+    ul = dk - ub
+    chains = [(d, d) for d in range(2)] + [(d, 1 - d) for d in range(2)]
+
+    def ring_rows(q, c, tt):
         fq = fs_of(q)
         w = upw if c == 0 else vaw
-        rows = pl.ds(pl.multiple_of(fq * bk + c * bh, bh), bh)
-        return w.at[tt, fq], bw.at[tt, rows, :]
-
-    def own(c):
-        return (up, val)[c], back.at[pl.ds(c * bh, bh), :]
+        rows = pl.ds(pl.multiple_of(fq * bk + c * bh + r * bq, bq), bq)
+        return w.at[tt, fq, pl.ds(pl.multiple_of(r * ub, 16), ul), :], bw.at[tt, rows, :]
+
+    def rep_rows(q, c, tt, rr):
+        fq = fs_of(q)
+        w = upw if c == 0 else vaw
+        rows = pl.ds(pl.multiple_of(fq * bk + c * bh + rr * bq, bq), bq)
+        return w.at[tt, fq, pl.ds(pl.multiple_of(rr * ul, 16), ub), :], bw.at[tt, rows, :]
+
+    def own_rows(c):
+        return (
+            (up, val)[c].at[pl.ds(pl.multiple_of(r * ub, 16), ul), :],
+            back.at[pl.ds(pl.multiple_of(c * bh + r * bq, bq), bq), :],
+        )
 
     def ring_send(s, d, c):
         q = ring(pos - sgn[d] * s)
-        dst = slots(q, c, t)
-        src = own(c) if s == 0 else dst
+        dst = ring_rows(q, c, t)
+        src = own_rows(c) if s == 0 else dst
         for i in range(2):
             send(src[i], dst[i], sem2(ring_s, d, c, s, i), nbr[d])
 
-    for d in range(2):
-        for c in range(2):
-            ring_send(0, d, c)
+    for d, c in chains:
+        ring_send(0, d, c)
 
     rows_own = pl.ds(pl.multiple_of(t * half_rows, half_rows), half_rows)
     rows_oth = pl.ds(pl.multiple_of((1 - t) * half_rows, half_rows), half_rows)
@@ -173,11 +187,13 @@
     send(vg, vgb.at[t], sem2(tok_s, 1), partner)
     send(mw, mwb.at[t], sem2(tok_s, 2), partner)
     send(mb, mbb.at[t], sem2(tok_s, 3), partner)
-    for c in range(2):
-        dst = slots(pos, c, t)
-        src = own(c)
-        for i in range(2):
-            send(src[i], dst[i], sem2(pw_s, 0, 0, c, i), partner)
+    own_slots = (
+        (up, upw.at[t, f]),
+        (val, vaw.at[t, f]),
+        (back, bw.at[t, pl.ds(pl.multiple_of(f * bk, bk), bk), :]),
+    )
+    for i, (src, dst) in enumerate(own_slots):
+        send(src, dst, sem2(tok_s, 4 + i), partner)
 
     hr, dr = hid.shape[0] // 2, fu // 2
 
@@ -221,36 +237,67 @@
     mbb[t] = mb[...]
 
     steps = n // 2
+    for i, ref in enumerate((xbuf.at[1 - t], vgb.at[1 - t], mwb.at[1 - t], mbb.at[1 - t])):
+        landed(ref, sem2(tok_s, i), partner)
+    xs = [xbuf[i].astype(F32) for i in range(2)]
+    tot = sum(jnp.sum(v * v, axis=1, keepdims=True) for v in xs)
+    sc = lax.rsqrt(tot / width + EPS)
+    for i in range(2):
+        nrm = (xs[i] * sc * g1[:, i * cd : (i + 1) * cd]).astype(BF)
+        for b in range(cd // dk):
+            nbuf[i * (cd // dk) + b] = nrm[:, b * dk : (b + 1) * dk]
+    oth = pl.ds(pl.multiple_of(f * bk, bk), bk)
+    for i, ref in enumerate((upw.at[1 - t, f], vaw.at[1 - t, f], bw.at[1 - t, oth, :])):
+        landed(ref, sem2(tok_s, 4 + i), partner)
+
+    def multiply(fq, first):
+        for tt in range(2):
+            for w, acc in ((upw, upacc), (vaw, vact)):
+                p = jnp.dot(nbuf[fq], w[tt, fq], preferred_element_type=F32)
+                acc[tt] = p if first else acc[tt] + p
+
+    multiply(f, True)
+
+    def complete(s):
+        got = [(d, c, ring(pos - sgn[d] * s)) for d, c in chains if s <= hops(d, c)]
+        for d, c, q in got:
+            for i, p in enumerate(rep_rows(q, c, t, 1 - r)):
+                landed(p, sem2(xr_s, s, d, c, i), xpeer)
+                send(p, p, sem2(px_s, s, d, c, i), partner)
+        for d, c, q in got:
+            for i, p in enumerate(ring_rows(q, c, 1 - t)):
+                landed(p, sem2(pw_s, s, d, c, i), partner)
+            for i, p in enumerate(rep_rows(q, c, 1 - t, 1 - r)):
+                landed(p, sem2(px_s, s, d, c, i), partner)
+        if s < steps:
+
+            @pl.loop(0, 2)
+            def _(j):
+                multiply(fs_of(ring(pos + s - 2 * s * j)), False)
+        else:
+            multiply(fs_of(ring(pos + s)), False)
+
     ks = list(range(1, n))
-    for s in range(1, steps):
-        for k in ks[: -(-(n - 1) // (steps - 1))]:
-            a2a_send(k)
-        ks = ks[-(-(n - 1) // (steps - 1)) :]
-        for d in range(2):
-            for c in range(2):
+    for s in range(1, steps + 1):
+        for d, c in chains:
+            if s <= hops(d, c):
                 q = ring(pos - sgn[d] * s)
-                land = slots(q, c, t)
+                land = ring_rows(q, c, t)
                 for i in range(2):
                     landed(land[i], sem2(ring_s, d, c, s - 1, i), nbr[d])
                 if s < hops(d, c):
                     ring_send(s, d, c)
+                for i, p in enumerate(rep_rows(q, c, t, r)):
+                    send(p, p, sem2(xr_s, s, d, c, i), xpeer)
                 for i in range(2):
                     send(land[i], land[i], sem2(pw_s, s, d, c, i), partner)
-        if s == 1:
-            for i, ref in enumerate((xbuf.at[1 - t], vgb.at[1 - t], mwb.at[1 - t], mbb.at[1 - t])):
-                landed(ref, sem2(tok_s, i), partner)
-            xs = [xbuf[i].astype(F32) for i in range(2)]
-            tot = sum(jnp.sum(v * v, axis=1, keepdims=True) for v in xs)
-            sc = lax.rsqrt(tot / width + EPS)
-            for i in range(2):
-                cols = slice(i * cd, (i + 1) * cd)
-                nbuf[:, cols] = (xs[i] * sc * g1[:, cols]).astype(BF)
-    for d in range(2):
-        q = ring(pos - sgn[d] * steps)
-        land = slots(q, d, t)
-        for i in range(2):
-            landed(land[i], sem2(ring_s, d, d, steps - 1, i), nbr[d])
-            send(land[i], land[i], sem2(pw_s, steps, d, d, i), partner)
+        if s < steps:
+            done = (n - 1) * s // (steps - 1)
+            while ks and ks[0] <= done:
+                a2a_send(ks.pop(0))
+        if s > 1:
+            complete(s - 1)
+
     def relay(k):
         g = lax.rem(f - k + n, n)
         hp, dp = hpiece(t, g, r), dpiece(t, g, r)
@@ -259,28 +306,19 @@
             send(p, p, sem2(x_s, k, i), xpeer)
             send(p, p, sem2(hd_s, k, i, 0), partner)
 
-    for c in range(2):
-        for i in range(2):
-            landed(slots(pos, c, 1 - t)[i], sem2(pw_s, 0, 0, c, i), partner)
-    for s in range(1, steps + 1):
-        for d in range(2):
-            for c in range(2):
-                if s <= hops(d, c):
-                    q = ring(pos - sgn[d] * s)
-                    for i in range(2):
-                        landed(slots(q, c, 1 - t)[i], sem2(pw_s, s, d, c, i), partner)
     for rr in range(2):
         send(hpiece(t, f, rr), hpiece(t, f, rr), sem2(hd_s, 0, 0, rr), partner)
         send(dpiece(t, f, rr), dpiece(t, f, rr), sem2(hd_s, 0, 1, rr), partner)
-    for k in range(1, n // 2):
+    first_relays = (n - 1) // 2
+    mid_relays = n - 2
+    for k in range(1, 1 + first_relays):
         relay(k)
+    complete(steps)
 
     @pl.loop(0, 2)
     def _(tt):
-        a = jnp.dot(nbuf[...], upw[tt].reshape(width, gwd), preferred_element_type=F32)
-        upact[tt] = gelu(a).astype(BF)
-        b = jnp.dot(nbuf[...], vaw[tt].reshape(width, gwd), preferred_element_type=F32)
-        vact[tt] = gelu(b)
+        upact[tt] = gelu(upacc[tt]).astype(BF)
+        vact[tt] = gelu(vact[tt])
 
     vs = [vact[i] for i in range(2)]
     tot = sum(jnp.sum(v * v, axis=1, keepdims=True) for v in vs)
@@ -302,6 +340,9 @@
                     upact[tt, rs_, cs].astype(F32) * mx
                 ).astype(BF)
 
+    for k in range(1 + first_relays, 1 + mid_relays):
+        relay(k)
+
     @pl.loop(0, 2)
     def _(tt):
         acc = jnp.dot(gated[...], bw[tt], preferred_element_type=F32)
@@ -317,11 +358,10 @@
         q = ring(pos - sgn[d] * s)
         send(ag.at[q, c], ag.at[q, c], sem2(ag_s, d, c, s), nbr[d])
 
-    for d in range(2):
-        for c in range(2):
-            ag_send(0, d, c)
-
-    for k in range(n // 2, n):
+    for d, c in chains:
+        ag_send(0, d, c)
+
+    for k in range(1 + mid_relays, n):
         relay(k)
     for k in range(1, n):
         g = lax.rem(f - k + n, n)
@@ -349,14 +389,22 @@
         for c in range(2):
             part[q, c] = jnp.dot(h, w[:, c * cd : (c + 1) * cd], preferred_element_type=F32)
 
+    def rs_send(s, d, c):
+        h = hops(d, c)
+        v = part[ring(pos + sgn[d] * (h - s)), c]
+        if s > 0:
+            landed(rsr.at[d, c, s - 1], sem2(rs_s, d, c, s - 1), nbr[d])
+            v = v + rsr[d, c, s - 1].astype(F32)
+        rss[d, c, s] = v.astype(BF)
+        send(rss.at[d, c, s], rsr.at[d, c, s], sem2(rs_s, d, c, s), nbr[d])
+
     for s in range(1, steps + 1):
-        for d in range(2):
-            for c in range(2):
-                if s <= hops(d, c):
-                    q = ring(pos - sgn[d] * s)
-                    landed(ag.at[q, c], sem2(ag_s, d, c, s - 1), nbr[d])
-                    if s < hops(d, c):
-                        ag_send(s, d, c)
+        for d, c in chains:
+            if s <= hops(d, c):
+                q = ring(pos - sgn[d] * s)
+                landed(ag.at[q, c], sem2(ag_s, d, c, s - 1), nbr[d])
+                if s < hops(d, c):
+                    ag_send(s, d, c)
         if s == 1:
 
             @pl.loop(0, 3)
@@ -369,19 +417,16 @@
                 mixer(ring(pos + s - 2 * s * j))
         else:
             mixer(ring(pos + s))
+        if s == steps - 1:
+            for d in range(2):
+                rs_send(0, d, 1 - d)
 
     for s in range(steps):
         for d in range(2):
-            for c in range(2):
-                h = hops(d, c)
-                if s < h:
-                    dest = ring(pos + sgn[d] * (h - s))
-                    v = part[dest, c]
-                    if s > 0:
-                        landed(rsr.at[d, c, s - 1], sem2(rs_s, d, c, s - 1), nbr[d])
-                        v = v + rsr[d, c, s - 1].astype(F32)
-                    rss[d, c, s] = v.astype(BF)
-                    send(rss.at[d, c, s], rsr.at[d, c, s], sem2(rs_s, d, c, s), nbr[d])
+            rs_send(s, d, d)
+        if s + 1 < steps - 1:
+            for d in range(2):
+                rs_send(s + 1, d, 1 - d)
     fin = []
     for c in range(2):
         v = part[pos, c]
@@ -417,7 +462,7 @@
     dma = pltpu.SemaphoreType.DMA
     scratch = [
         v((2, hrows, cd), BF),
-        v((hrows, 2 * cd), BF),
+        v((n, hrows, dk), BF),
         v((2, n, dk, gwd), BF),
         v((2, n, dk, gwd), BF),
         v((2, n * bk, cd), BF),
@@ -426,8 +471,9 @@
         v((2, 1, gwd), F32),
         v((2,) + mw.shape, BF),
         v((2,) + mb.shape, F32),
+        v((2, hrows, gwd), F32),
+        v((2, hrows, gwd), F32),
         v((2, hrows, gwd), BF),
-        v((2, hrows, gwd), F32),
         v((hrows, 2 * gwd), BF),
         v((2, hrows, cd), BF),
         v((n, 2, hrows, cd), BF),
@@ -436,9 +482,10 @@
         v((2, 2, steps, hrows, cd), BF),
         v((2, hrows, cd), BF),
         v((hrows, cd), BF),
-        dma((2, 4)),
+        dma((2, 7)),
         dma((2, 2, 2, steps, 2)),
-        dma((1,)),
+        dma((2, steps + 1, 2, 2, 2)),
+        dma((2, steps + 1, 2, 2, 2)),
         dma((2, steps + 1, 2, 2, 2)),
         dma((2, n, 2)),
         dma((2, n, 2)),
@@ -570,7 +617,7 @@
     fu = hid.shape[1] // n
     if mesh.shape["rep"] != 2 or mesh.shape["tp"] != 2 or n % 2 or n < 4:
         return False
-    if hrows % mw.shape[1] or fu % 256 or down.shape[1] % 128 or back.shape[0] % 32:
+    if hrows % mw.shape[1] or fu % 256 or down.shape[1] % 128 or up.shape[0] % 256 or back.shape[0] % 64:
         return False
     held = 2 * (up.size * 2 + back.size + hid.size + down.size)
     held += 4 * n * (up.size * 2 + back.size) + 4 * (hid.size + down.size)

time: 240 us -> 214 us (0.89)
  Pallas kernels: 237 us -> 212 us
    pallas_call x1, Pallas kernels: 237 us -> 212 us  [fused(): pl.pallas_call(functools.partial(kernel, dims), out_shape=jax.ShapeDtypeS...]
where the time goes in v2:
time: 214 us
  Pallas kernels  212 us (99%)
    pallas_call x1, Pallas kernels, fused(): pl.pallas_call(functools.partial(kernel, dims), out_shape=jax.ShapeDtypeS...  212 us

profile of v2, /device:TPU:0, one launch (start us, length us, event | category | flops | bytes accessed | tf_op | source)
XLA Modules:
  0.0 214.0 jit_solution(17998664731727004469)
XLA Ops:
  0.0 212.1 %shard_map.118 = bf16[256,1024]{1,0:T(8,128)(2,1)} custom-call(bf16[256,1024]{1,0:T(8,128)(2,1)} %tok.1, f32[1,2048]{1,0:T(1,128)} %bitcast.4, bf16[256,512]{1,0:T(8,128)(2,1)} %up.1, bf16[256,512]{1,0:T(8,128)(2,1)} %val.1, f32[1,512]{1,0:T(1,128)} %bitcast.7, bf16[4,128,128]{2,1,0:T(8,128)(2,1)} %mw.1, f32[4,128]{1,0:T(4,128)} %mb.1, ...), custom_call_target="tpu_custom_call" | custom-call | tf_op jit(solution)/shard_map/pallas_call | solution.py:497
  212.1 1.9 copy.14

commit v3 on v2

--- a/solution.py
+++ b/solution.py
@@ -149,7 +149,7 @@
 
     bh = bk // 2
     bq = bh // 2
-    ub = 5 * dk // 256 * 16
+    ub = dk // 2
     ul = dk - ub
     chains = [(d, d) for d in range(2)] + [(d, 1 - d) for d in range(2)]
 
@@ -310,7 +310,6 @@
         send(hpiece(t, f, rr), hpiece(t, f, rr), sem2(hd_s, 0, 0, rr), partner)
         send(dpiece(t, f, rr), dpiece(t, f, rr), sem2(hd_s, 0, 1, rr), partner)
     first_relays = (n - 1) // 2
-    mid_relays = n - 2
     for k in range(1, 1 + first_relays):
         relay(k)
     complete(steps)
@@ -340,9 +339,6 @@
                     upact[tt, rs_, cs].astype(F32) * mx
                 ).astype(BF)
 
-    for k in range(1 + first_relays, 1 + mid_relays):
-        relay(k)
-
     @pl.loop(0, 2)
     def _(tt):
         acc = jnp.dot(gated[...], bw[tt], preferred_element_type=F32)
@@ -361,8 +357,18 @@
     for d, c in chains:
         ag_send(0, d, c)
 
-    for k in range(1 + mid_relays, n):
+    def ag_step(s):
+        for d, c in chains:
+            if s <= hops(d, c):
+                q = ring(pos - sgn[d] * s)
+                landed(ag.at[q, c], sem2(ag_s, d, c, s - 1), nbr[d])
+                if s < hops(d, c):
+                    ag_send(s, d, c)
+
+    for k in range(1 + first_relays, n):
         relay(k)
+    for s in range(1, steps - 1):
+        ag_step(s)
     for k in range(1, n):
         g = lax.rem(f - k + n, n)
         for i, p in enumerate((hpiece(t, g, 1 - r), dpiece(t, g, 1 - r))):
@@ -398,28 +404,21 @@
         rss[d, c, s] = v.astype(BF)
         send(rss.at[d, c, s], rsr.at[d, c, s], sem2(rs_s, d, c, s), nbr[d])
 
-    for s in range(1, steps + 1):
-        for d, c in chains:
-            if s <= hops(d, c):
-                q = ring(pos - sgn[d] * s)
-                landed(ag.at[q, c], sem2(ag_s, d, c, s - 1), nbr[d])
-                if s < hops(d, c):
-                    ag_send(s, d, c)
-        if s == 1:
-
-            @pl.loop(0, 3)
-            def _(j):
-                mixer(ring(pos + j - 1))
-        elif s < steps:
-
-            @pl.loop(0, 2)
-            def _(j):
-                mixer(ring(pos + s - 2 * s * j))
-        else:
-            mixer(ring(pos + s))
-        if s == steps - 1:
-            for d in range(2):
-                rs_send(0, d, 1 - d)
+    @pl.loop(0, 3)
+    def _(j):
+        mixer(ring(pos + j - 1))
+
+    ag_step(steps - 1)
+    for s in range(2, steps):
+
+        @pl.loop(0, 2)
+        def _(j):
+            mixer(ring(pos + s - 2 * s * j))
+
+    for d in range(2):
+        rs_send(0, d, 1 - d)
+    ag_step(steps)
+    mixer(ring(pos + steps))
 
     for s in range(steps):
         for d in range(2):

time: 214 us -> 190 us (0.89)
  Pallas kernels: 212 us -> 188 us
    pallas_call x1, Pallas kernels: 212 us -> 188 us  [fused(): pl.pallas_call(functools.partial(kernel, dims), out_shape=jax.ShapeDtypeS...]
where the time goes in v3:
time: 190 us
  Pallas kernels  188 us (99%)
    pallas_call x1, Pallas kernels, fused(): pl.pallas_call(functools.partial(kernel, dims), out_shape=jax.ShapeDtypeS...  188 us

profile of v3, /device:TPU:0, one launch (start us, length us, event | category | flops | bytes accessed | tf_op | source)
XLA Modules:
  0.0 190.0 jit_solution(13552728593103893726)
XLA Ops:
  0.0 188.1 %shard_map.118 = bf16[256,1024]{1,0:T(8,128)(2,1)} custom-call(bf16[256,1024]{1,0:T(8,128)(2,1)} %tok.1, f32[1,2048]{1,0:T(1,128)} %bitcast.4, bf16[256,512]{1,0:T(8,128)(2,1)} %up.1, bf16[256,512]{1,0:T(8,128)(2,1)} %val.1, f32[1,512]{1,0:T(1,128)} %bitcast.7, bf16[4,128,128]{2,1,0:T(8,128)(2,1)} %mw.1, f32[4,128]{1,0:T(4,128)} %mb.1, ...), custom_call_target="tpu_custom_call" | custom-call | tf_op jit(solution)/shard_map/pallas_call | solution.py:496
  188.1 1.9 copy.14

commit v4 on v3

--- a/solution.py
+++ b/solution.py
@@ -89,6 +89,7 @@
     ag_s,
     rs_s,
     y_s,
+    own_s,
 ):
     n, half_rows, cd, span = dims
     dk, gwd = up.shape
@@ -221,16 +222,29 @@
             dev,
         )
 
+    a2a_send(1)
+
     for c in range(2):
         w = (upw, vaw)[c]
         w[t, f] = (up, val)[c][...]
     bw[t, pl.ds(pl.multiple_of(f * bk, bk), bk), :] = back[...]
     own_cols = pl.ds(pl.multiple_of(f * fu, fu), fu)
+    local = []
     for rr in range(2):
-        hw[t, f, rr] = hid[rr * hr : (rr + 1) * hr, own_cols]
-        dw[t, rr, :, pl.ds(pl.multiple_of(f * dcol, dcol), dcol)] = down[
-            pl.ds(pl.multiple_of(f * fu + rr * dr, dr), dr), :
-        ]
+        local.append(
+            pltpu.make_async_copy(
+                hid.at[pl.ds(rr * hr, hr), own_cols], hpiece(t, f, rr), own_s.at[rr, 0]
+            )
+        )
+        local.append(
+            pltpu.make_async_copy(
+                down.at[pl.ds(pl.multiple_of(f * fu + rr * dr, dr), dr), :],
+                dpiece(t, f, rr),
+                own_s.at[rr, 1],
+            )
+        )
+    for cp in local:
+        cp.start()
     xbuf[t] = tok[rows_own, :]
     vgb[t] = vg[...]
     mwb[t] = mw[...]
@@ -277,7 +291,7 @@
         else:
             multiply(fs_of(ring(pos + s)), False)
 
-    ks = list(range(1, n))
+    ks = list(range(2, n))
     for s in range(1, steps + 1):
         for d, c in chains:
             if s <= hops(d, c):
@@ -291,12 +305,13 @@
                     send(p, p, sem2(xr_s, s, d, c, i), xpeer)
                 for i in range(2):
                     send(land[i], land[i], sem2(pw_s, s, d, c, i), partner)
-        if s < steps:
-            done = (n - 1) * s // (steps - 1)
-            while ks and ks[0] <= done:
-                a2a_send(ks.pop(0))
-        if s > 1:
-            complete(s - 1)
+        if s < steps - 1:
+            a2a_send(ks.pop(0))
+        elif s == steps - 1:
+            for k in ks:
+                a2a_send(k)
+        if s > 2:
+            complete(s - 2)
 
     def relay(k):
         g = lax.rem(f - k + n, n)
@@ -306,12 +321,15 @@
             send(p, p, sem2(x_s, k, i), xpeer)
             send(p, p, sem2(hd_s, k, i, 0), partner)
 
+    for cp in local:
+        cp.wait()
     for rr in range(2):
         send(hpiece(t, f, rr), hpiece(t, f, rr), sem2(hd_s, 0, 0, rr), partner)
         send(dpiece(t, f, rr), dpiece(t, f, rr), sem2(hd_s, 0, 1, rr), partner)
     first_relays = (n - 1) // 2
     for k in range(1, 1 + first_relays):
         relay(k)
+    complete(steps - 1)
     complete(steps)
 
     @pl.loop(0, 2)
@@ -404,28 +422,30 @@
         rss[d, c, s] = v.astype(BF)
         send(rss.at[d, c, s], rsr.at[d, c, s], sem2(rs_s, d, c, s), nbr[d])
 
-    @pl.loop(0, 3)
-    def _(j):
-        mixer(ring(pos + j - 1))
-
     ag_step(steps - 1)
-    for s in range(2, steps):
-
+
+    def mixer_pair(s):
         @pl.loop(0, 2)
         def _(j):
             mixer(ring(pos + s - 2 * s * j))
 
+    mixer_pair(steps - 1)
     for d in range(2):
         rs_send(0, d, 1 - d)
     ag_step(steps)
     mixer(ring(pos + steps))
-
     for s in range(steps):
         for d in range(2):
             rs_send(s, d, d)
+        if s + 1 < steps:
+            if steps - 2 - s > 0:
+                mixer_pair(steps - 2 - s)
+            else:
+                mixer(pos)
         if s + 1 < steps - 1:
             for d in range(2):
                 rs_send(s + 1, d, 1 - d)
+
     fin = []
     for c in range(2):
         v = part[pos, c]
@@ -492,11 +512,14 @@
         dma((2, 2, 2, steps)),
         dma((2, 2, 2, steps)),
         dma((2, 1)),
+        dma((2, 2)),
     ]
     return pl.pallas_call(
         functools.partial(kernel, dims),
         out_shape=jax.ShapeDtypeStruct((rows, cd), BF),
-        in_specs=[pl.BlockSpec(memory_space=pltpu.VMEM)] * 12,
+        in_specs=[
+            pl.BlockSpec(memory_space=pltpu.HBM if i in (9, 10) else pltpu.VMEM) for i in range(12)
+        ],
         out_specs=pl.BlockSpec(memory_space=pltpu.VMEM),
         scratch_shapes=scratch,
         compiler_params=pltpu.CompilerParams(

time: 190 us -> 179 us (0.942)
  Pallas kernels: 188 us -> 176 us
    pallas_call x1, Pallas kernels: 188 us -> 176 us  [fused(): pl.pallas_call(functools.partial(kernel, dims), out_shape=jax.ShapeDtypeS...]
where the time goes in v4:
time: 179 us; the launch traced here: 178 us
  Pallas kernels  176 us (98%)
  local copies, waits for them, and re-layouts  1.87 us (1%)
    pallas_call x1, Pallas kernels, fused(): pl.pallas_call(functools.partial(kernel, dims), out_shape=jax.ShapeDtypeS...  176 us

profile of v4, /device:TPU:0, one launch (start us, length us, event | category | flops | bytes accessed | tf_op | source)
XLA Modules:
  0.0 178.0 jit_solution(8698791486673563972)
XLA Ops:
  0.0 176.1 %shard_map.118 = bf16[256,1024]{1,0:T(8,128)(2,1)} custom-call(bf16[256,1024]{1,0:T(8,128)(2,1)} %tok.1, f32[1,2048]{1,0:T(1,128)} %bitcast.4, bf16[256,512]{1,0:T(8,128)(2,1)} %up.1, bf16[256,512]{1,0:T(8,128)(2,1)} %val.1, f32[1,512]{1,0:T(1,128)} %bitcast.7, bf16[4,128,128]{2,1,0:T(8,128)(2,1)} %mw.1, f32[4,128]{1,0:T(4,128)} %mb.1, ...), custom_call_target="tpu_custom_call" | custom-call | tf_op jit(solution)/shard_map/pallas_call | solution.py:517
  176.1 1.9 %copy.14 = bf16[256,1024]{1,0:T(8,128)(2,1)} copy(bf16[256,1024]{1,0:T(8,128)(2,1)} %shard_map.118) | data formatting | bytes 1048576
